TPU v7x, 32 devices: a whole 2x2x4 slice. The times are simulated.
32 devices in a mesh: sp: 16 (over z, y, x), tp: 2 (over core).
Axes of the slice: x: 2, y: 2, z: 4, core: 2. Of those that a mesh axis runs over, the one named last changes fastest.
Arguments:
- latent: bfloat16 [4096, 2048], P(('sp', 'tp')), may hold values from -6 to 6
- cond: float32 [2048], replicated, may hold values from -6 to 6
- ctx_mod: float32 [2048], replicated, may hold values from -6 to 6
- context: bfloat16 [512, 2048], P(('sp', 'tp')), may hold values from -6 to 6
- shift_w: float32 [2048, 2048], P('sp', 'tp'), may hold values from -0.125 to 0.125
- scale_w: float32 [2048, 2048], P('sp', 'tp'), may hold values from -0.125 to 0.125
- gate_w: float32 [2048, 2048], P('sp', 'tp'), may hold values from -0.125 to 0.125
- norm_gain: float32 [2048], replicated, may hold values from 0.1 to 1.9
- w_qn: bfloat16 [2048, 2048], P(None, 'tp'), may hold values from -0.125 to 0.125
- w_qr: bfloat16 [2048, 1024], P(None, 'tp'), may hold values from -0.13258252 to 0.13258252
- w_kv_down: bfloat16 [2048, 512], replicated, may hold values from -0.125 to 0.125
- w_rope_key: bfloat16 [2048, 64], replicated, may hold values from -0.13258252 to 0.13258252
- kv_gain: float32 [512], replicated, may hold values from 0.1 to 1.9
- w_key_up: bfloat16 [512, 2048], P(None, 'tp'), may hold values from -0.66015625 to 0.66015625
- w_value_up: bfloat16 [512, 2048], P(None, 'tp'), may hold values from -0.25 to 0.25
- ctx_bias: float32 [16], P('tp'), may hold values from 2 to 3.5
- w_out: bfloat16 [2048, 2048], P('tp'), may hold values from -0.52734375 to 0.52734375
Outputs:
- mixed: bfloat16 [4096, 2048], P(('sp', 'tp'))
All inputs are finite; a program needn't handle non-finite values.
Results may differ from a plain program's by a relative error of at most 0.018.
Values may be sent and summed in bfloat16 or wider, within the bound.
A program may use at most 128 MiB of HBM per device.

v0:
```python
import jax
import jax.numpy as jnp
from jax import lax
from jax.sharding import PartitionSpec as P

GRID_W = 128
EPS = 1e-06
ROPE_BASE = 10000.0


def modulate(rows_in, gain, shift, scale):
    values = rows_in.astype(jnp.float32)
    normed = values * lax.rsqrt(jnp.mean(values * values, axis=-1, keepdims=True) + EPS)
    return (normed * gain * (1.0 + scale) + shift).astype(jnp.bfloat16)


def compress(rows_in, w_kv_down, kv_gain):
    inner = jnp.dot(rows_in, w_kv_down, preferred_element_type=jnp.float32)
    normed = inner * lax.rsqrt(jnp.mean(inner * inner, axis=-1, keepdims=True) + EPS)
    return (normed * kv_gain).astype(jnp.bfloat16)


def angles(positions, rope_dim):
    quarter = rope_dim // 4
    inverse = ROPE_BASE ** (-jnp.arange(quarter, dtype=jnp.float32) / quarter)
    row = (positions // GRID_W).astype(jnp.float32)
    column = (positions % GRID_W).astype(jnp.float32)
    return jnp.concatenate(
        [row[:, None] * inverse[None, :], column[:, None] * inverse[None, :]], axis=-1
    )


def rotate(values, angle):
    pairs = values.reshape(values.shape[:-1] + (values.shape[-1] // 2, 2))
    first = pairs[..., 0]
    second = pairs[..., 1]
    cosine = jnp.cos(angle)
    sine = jnp.sin(angle)
    turned = jnp.stack([first * cosine - second * sine, first * sine + second * cosine], axis=-1)
    return turned.reshape(values.shape)


def body(
    latent,
    cond,
    ctx_mod,
    context,
    shift_w,
    scale_w,
    gate_w,
    norm_gain,
    w_qn,
    w_qr,
    w_kv_down,
    w_rope_key,
    kv_gain,
    w_key_up,
    w_value_up,
    ctx_bias,
    w_out,
):
    n_tp = lax.axis_size("tp")
    sp_index = lax.axis_index("sp")
    tp_index = lax.axis_index("tp")
    rows = latent.shape[0]
    ctx_rows = context.shape[0]
    width = latent.shape[1]
    tok_dev = rows * n_tp
    heads_dev = ctx_bias.shape[0]
    nope = w_key_up.shape[1] // heads_dev
    vsize = w_value_up.shape[1] // heads_dev
    rope = w_rope_key.shape[1]
    period = rows + ctx_rows
    factor = (nope + rope) ** (-0.5)
    pair = jnp.stack([jax.nn.silu(cond), jax.nn.silu(ctx_mod)])
    feat_block = shift_w.shape[0]
    pair_block = lax.dynamic_slice_in_dim(pair, sp_index * feat_block, feat_block, 1)
    partials = tuple(
        (
            jnp.dot(pair_block, weight, precision=lax.Precision.HIGHEST)
            for weight in (shift_w, scale_w, gate_w)
        )
    )
    columns = shift_w.shape[1]
    placed = tuple(
        (
            lax.dynamic_update_slice_in_dim(
                jnp.zeros((2, width), jnp.float32), part, tp_index * columns, 1
            )
            for part in partials
        )
    )
    shift, scale, gate = lax.psum((placed[0], placed[1], placed[2]), ("sp", "tp"))
    h_rows = modulate(latent, norm_gain, shift[0], scale[0])
    h_ctx = modulate(context, norm_gain, shift[1], scale[1])
    own_positions = sp_index * tok_dev + tp_index * rows + jnp.arange(rows, dtype=jnp.int32)
    own_latents = jnp.concatenate(
        [compress(h_rows, w_kv_down, kv_gain), compress(h_ctx, w_kv_down, kv_gain)], axis=0
    )
    rope_rows = rotate(
        jnp.dot(h_rows, w_rope_key, preferred_element_type=jnp.float32), angles(own_positions, rope)
    ).astype(jnp.bfloat16)
    rope_ctx = jnp.dot(h_ctx, w_rope_key, preferred_element_type=jnp.float32).astype(jnp.bfloat16)
    own_rope = jnp.concatenate([rope_rows, rope_ctx], axis=0)
    piece = lax.all_gather(h_rows, "tp", axis=0, tiled=True)
    count = piece.shape[0]
    nope_part = jnp.dot(piece, w_qn, preferred_element_type=jnp.float32).astype(jnp.bfloat16)
    places = sp_index * tok_dev + jnp.arange(count, dtype=jnp.int32)
    rope_part = jnp.dot(piece, w_qr, preferred_element_type=jnp.float32).reshape(
        count, heads_dev, rope
    )
    rope_part = rotate(rope_part, angles(places, rope)[:, None, :]).reshape(count, heads_dev * rope)
    queries = jnp.concatenate([nope_part, rope_part.astype(jnp.bfloat16)], axis=1)
    query_nope = queries[:, : heads_dev * nope].reshape(tok_dev, heads_dev, nope)
    query_rope = queries[:, heads_dev * nope :].reshape(tok_dev, heads_dev, rope)

    def fold_keys(carry, keys, values, rope_keys):
        best, total, accum = carry
        count = rope_keys.shape[0]
        keys = keys.reshape(count, heads_dev, nope)
        values = values.reshape(count, heads_dev, vsize)
        scores = jnp.einsum("qhd,khd->hqk", query_nope, keys, preferred_element_type=jnp.float32)
        scores = scores + jnp.einsum(
            "qhr,kr->hqk", query_rope, rope_keys, preferred_element_type=jnp.float32
        )
        index = jnp.arange(count, dtype=jnp.int32)
        is_ctx = (index % period >= rows).astype(jnp.float32)
        scores = scores * factor + ctx_bias[:, None, None] * is_ctx[None, None, :]
        new_best = jnp.maximum(best, jnp.max(scores, axis=-1))
        weights = jnp.exp(scores - new_best[..., None])
        total = jnp.sum(weights, axis=-1)
        accum = jnp.einsum(
            "hqk,khd->hqd", weights.astype(jnp.bfloat16), values, preferred_element_type=jnp.float32
        )
        return (new_best, total, accum)

    start_carry = (
        jnp.full((heads_dev, tok_dev), -1e30, jnp.float32),
        jnp.zeros((heads_dev, tok_dev), jnp.float32),
        jnp.zeros((heads_dev, tok_dev, vsize), jnp.float32),
    )
    pieces = (
        lax.all_gather(own_latents, ("sp", "tp"), axis=0, tiled=True),
        lax.all_gather(own_rope, ("sp", "tp"), axis=0, tiled=True),
    )
    keys = jnp.dot(pieces[0], w_key_up, preferred_element_type=jnp.float32).astype(jnp.bfloat16)
    values = jnp.dot(pieces[0], w_value_up, preferred_element_type=jnp.float32).astype(jnp.bfloat16)
    best, total, accum = fold_keys(start_carry, keys, values, pieces[1])
    attended = (accum / total[..., None]).astype(jnp.bfloat16)
    attended = jnp.transpose(attended, (1, 0, 2)).reshape(tok_dev, heads_dev * vsize)
    part = attended
    branch = lax.psum_scatter(
        jnp.dot(part, w_out, preferred_element_type=jnp.float32).astype(jnp.bfloat16),
        "tp",
        scatter_dimension=0,
        tiled=True,
    ).astype(jnp.float32)
    return (latent.astype(jnp.float32) + gate[0] * branch).astype(jnp.bfloat16)


def solution(mesh):
    placed = (
        P(("sp", "tp"), None),
        P(),
        P(),
        P(("sp", "tp"), None),
        P("sp", "tp"),
        P("sp", "tp"),
        P("sp", "tp"),
        P(),
        P(None, "tp"),
        P(None, "tp"),
        P(),
        P(),
        P(),
        P(None, "tp"),
        P(None, "tp"),
        P("tp"),
        P("tp", None),
    )
    return jax.shard_map(
        body, mesh=mesh, in_specs=placed, out_specs=P(("sp", "tp"), None), check_vma=False
    )
```

profile of v0, /device:TPU:0, one launch (start us, length us, event | category | flops | bytes accessed | tf_op | source)
XLA Modules:
  0.0 253.4 jit_solution(1283834722461088093)
XLA Ops:
  6.5 0.0 copy-start
  6.5 0.0 copy-start.6
  6.5 0.0 copy-start.5
  6.5 0.0 copy-start.4
  6.5 0.0 copy-start.7
  6.5 0.0 all-gather.4.cloned.1.call-start
  6.6 0.9 divide_multiply_fusion.1
  7.5 0.7 divide_multiply_fusion
  8.2 1.2 fusion.17
  9.4 1.4 convolution_dynamic-update-slice_fusion.1
  10.9 1.4 convolution_dynamic-update-slice_fusion.2
  12.3 1.4 convolution_dynamic-update-slice_fusion
  13.8 42.5 %all-reduce = (f32[2,2048]{1,0:T(2,128)S(1)}, f32[2,2048]{1,0:T(2,128)S(1)}, f32[2,2048]{1,0:T(2,128)S(1)}) all-reduce(f32[2,2048]{1,0:T(2,128)S(1)} %convolution_dynamic-update-slice_fusion, f32[2,2048]{1,0:T(2,128)S(1)} %convolution_dynamic-update-slice_fusion.1, ...), channel_id=1, replica_groups=mesh['sp'=16,'tp'=2] {'sp','tp'}, use_global_device_ids=true, to_apply=%region_3.4 | all-reduce | flops 12288 | bytes 98304 | tf_op jit(solution)/shard_map/psum | solution.py:93
  56.3 2.1 fusion.21
  58.4 0.0 all-gather.4.cloned.1.call-update
  58.4 0.0 all-gather.6.cloned.1.call-start
  58.5 2.3 multiply_reduce_fusion
  60.8 1.0 fusion.26
  61.8 2.2 multiply_reduce_fusion.1
  64.0 0.8 multiply_convert_fusion.1
  64.7 0.8 multiply_convert_fusion
  65.5 0.7 pad_maximum_fusion.1
  66.2 0.0 all-gather.6.cloned.1.call-update
  66.2 0.0 reduce-scatter.2.cloned.1.call-start
  66.3 0.1 multiply_bitcast_fusion.1
  66.4 0.0 copy-done.4
  66.4 1.3 fusion.55
  67.8 0.1 subtract_convert_fusion.1
  67.9 0.0 copy-done.6
  67.9 0.0 copy-done.5
  67.9 0.2 convolution_convert_fusion.4
  68.1 0.1 copy.49
  68.3 44.1 %all-gather = bf16[32,144,64]{1,2,0:T(8,128)(2,1)S(1)} all-gather(bf16[1,144,64]{1,2,0:T(8,128)(2,1)S(1)} %maximum_bitcast_fusion), channel_id=1, replica_groups=mesh['sp'=16,'tp'=2] {'sp','tp'}, dimensions={0}, use_global_device_ids=true | all-gather | bytes 608256 | tf_op jit(solution)/shard_map/all_gather | solution.py:144
  112.4 0.6 copy.50
  113.0 2.5 reshape.383
  115.5 0.1 broadcast_multiply_fusion.2
  115.6 0.1 fusion.32
  115.7 0.0 copy-done.7
  115.7 0.1 broadcast_multiply_fusion
  115.8 0.0 all-gather.4.cloned.1.call-done
  115.8 0.0 copy-done
  115.8 2.5 fusion.56
  118.3 0.3 reshape_reshape.4
  118.6 0.7 subtract_convert_fusion
  119.3 0.6 pad_maximum_fusion
  119.9 0.1 convert_element_type.105
  120.0 3.8 %fusion.10 = bf16[32,8,8,128]{3,2,1,0:T(8,128)(2,1)S(1)} fusion(bf16[256,2048]{1,0:T(8,128)(2,1)} %all-gather.4.cloned.1.call-done, bf16[2048,1024]{1,0:T(8,128)(2,1)} %param.25), kind=kOutput, calls=%fused_computation.16 | convolution fusion | flops 1074003968 | bytes 5767168 | tf_op jit(solution)/shard_map/dot_general | solution.py:107
  123.8 12.6 %all-gather.6.cloned.1.call-done = bf16[4608,512]{1,0:T(8,128)(2,1)} async-done(((bf16[144,512]{1,0:T(8,128)(2,1)}), bf16[4608,512]{1,0:T(8,128)(2,1)}) %all-gather.6.cloned.1.call-update) | async-done | bytes 4718608 | tf_op jit(solution)/shard_map/all_gather | solution.py:143
  136.4 9.5 %convolution_convert_fusion.1 = bf16[4608,1024]{0,1:T(8,128)(2,1)} fusion(bf16[4608,512]{1,0:T(8,128)(2,1)} %all-gather.6.cloned.1.call-done, bf16[512,1024]{1,0:T(8,128)(2,1)} %param.30), kind=kOutput, calls=%fused_computation.9 | convolution fusion | flops 4836556800 | bytes 15204352 | tf_op jit(solution)/shard_map/dot_general | solution.py:146
  145.9 0.0 copy-start.3
  145.9 18.4 %fusion.23 = f32[8,256,4608]{2,1,0:T(8,128)} fusion(bf16[4608,8,128]{0,2,1:T(8,128)(2,1)} %bitcast.68, bf16[32,8,8,128]{3,2,1,0:T(8,128)(2,1)S(1)} %fusion.10), kind=kOutput, calls=%fused_computation.29 | convolution fusion | flops 2415919104 | bytes 47710208 | tf_op jit(solution)/shard_map/qhd,khd->hqk/dot_general | solution.py:122
  164.3 0.0 copy-done.3
  164.3 27.8 %fusion.54 = (f32[8,256]{1,0:T(8,128)S(1)}, f32[8,256,4608]{2,1,0:T(8,128)}) fusion(f32[8,4608]{1,0:T(8,128)S(1)} %broadcast_multiply_fusion, f32[8,256,4608]{2,1,0:T(8,128)} %fusion.23, bf16[4608,64,1]{0,1,2:T(8,128)(2,1)S(1)} %copy-done.3, bf16[256,8,64]{0,2,1:T(8,128)(2,1)S(1)} %convert_element_type.105), kind=kOutput, calls=%fused_computation.103 | convolution fusion | flops 1245706240 | bytes 76505088 | tf_op jit(solution)/shard_map/qhr,kr->hqk/dot_general | solution.py:123
  192.1 16.3 %fusion.2 = f32[8,256]{1,0:T(8,128)S(1)} fusion(f32[8,256,4608]{2,1,0:T(8,128)} %get-tuple-element.29, f32[8,256]{1,0:T(8,128)S(1)} %broadcast_maximum_fusion), kind=kLoop, calls=%fused_computation.4 | loop fusion | flops 18872320 | bytes 37765120 | tf_op jit(solution)/shard_map/reduce_sum | solution.py:131
  208.4 0.0 copy-done.9
  208.4 9.9 %convolution_convert_fusion = bf16[4608,1024]{0,1:T(8,128)(2,1)} fusion(bf16[4608,512]{1,0:T(8,128)(2,1)} %all-gather.6.cloned.1.call-done, bf16[512,1024]{1,0:T(8,128)(2,1)S(1)} %copy-done.9), kind=kOutput, calls=%fused_computation.8 | convolution fusion | flops 4836556800 | bytes 15204352 | tf_op jit(solution)/shard_map/dot_general | solution.py:147
  218.3 17.5 %fusion.14 = bf16[256,8,128]{0,2,1:T(8,128)(2,1)S(1)} fusion(bf16[4608,8,128]{0,2,1:T(8,128)(2,1)} %bitcast.67, f32[8,256,4608]{2,1,0:T(8,128)} %get-tuple-element.29, f32[8,256]{1,0:T(8,128)S(1)} %broadcast_maximum_fusion, f32[256,8]{0,1:T(8,128)S(1)} %bitcast.70), kind=kOutput, calls=%fused_computation.18 | convolution fusion | flops 2435317760 | bytes 47726592 | tf_op jit(solution)/shard_map/hqk,khd->hqd/dot_general | solution.py:132
  235.7 0.0 copy-done.8
  235.8 2.2 convolution_convert_fusion.2
  238.0 0.0 reduce-scatter.2.cloned.1.call-update
  238.0 6.8 %reduce-scatter.2.cloned.1.call-done = bf16[128,2048]{1,0:T(8,128)(2,1)} async-done(((bf16[256,2048]{1,0:T(8,128)(2,1)}), bf16[128,2048]{1,0:T(8,128)(2,1)}) %reduce-scatter.2.cloned.1.call-update) | async-done | bytes 524304 | tf_op jit(solution)/shard_map/reduce_scatter | solution.py:152
  244.9 0.0 copy-done.2
  244.9 2.0 fusion.22
  246.9 0.0 copy-done.1
  (22 shorter events, 0.2 us)
Async XLA Ops:
  6.5 109.3 %copy-start = (bf16[2048,512]{1,0:T(8,128)(2,1)S(1)}, bf16[2048,512]{1,0:T(8,128)(2,1)}, u32[]{:S(2)}) copy-start(bf16[2048,512]{1,0:T(8,128)(2,1)} %param.26) | copy-start | bytes 6291460
  6.5 61.4 %copy-start.6 = (f32[2048]{0:T(1024)S(1)}, f32[2048]{0:T(1024)}, u32[]{:S(2)}) copy-start(f32[2048]{0:T(1024)} %param.24) | copy-start | bytes 24580
  6.5 61.4 %copy-start.5 = (bf16[16,2048]{1,0:T(8,128)(2,1)S(1)}, bf16[16,2048]{1,0:T(8,128)(2,1)}, u32[]{:S(2)}) copy-start(bf16[16,2048]{1,0:T(8,128)(2,1)} %param.20) | copy-start | bytes 196612
  6.5 59.8 %copy-start.4 = (bf16[2048,64]{0,1:T(8,128)(2,1)S(1)}, bf16[2048,64]{0,1:T(8,128)(2,1)}, u32[]{:S(2)}) copy-start(bf16[2048,64]{0,1:T(8,128)(2,1)} %param.28) | copy-start | bytes 786436
  6.5 109.2 %copy-start.7 = (f32[8]{0:T(128)S(1)}, f32[8]{0:T(128)}, u32[]{:S(2)}) copy-start(f32[8]{0:T(128)} %param.32) | copy-start | bytes 100
  6.5 109.3 %all-gather.4.cloned.1.call-start = ((), (), s32[]{:S(2)}) async-start(), calls=%async_computation.1 | async-start | bytes 1572864 | tf_op jit(solution)/shard_map/all_gather | solution.py:105
  58.4 78.0 %all-gather.6.cloned.1.call-start = ((), (), s32[]{:S(2)}) async-start(), calls=%async_computation.2 | async-start | bytes 4866048 | tf_op jit(solution)/shard_map/all_gather | solution.py:143
  66.2 178.6 %reduce-scatter.2.cloned.1.call-start = ((), (), s32[]{:S(2)}) async-start(), calls=%async_computation.3 | async-start | bytes 1572864 | tf_op jit(solution)/shard_map/reduce_scatter | solution.py:152
  145.9 18.4 %copy-start.3 = (bf16[4608,64,1]{0,1,2:T(8,128)(2,1)S(1)}, bf16[4608,64,1]{0,1,2:T(8,128)(2,1)}, u32[]{:S(2)}) copy-start(bf16[4608,64,1]{0,1,2:T(8,128)(2,1)} %reshape.383) | copy-start | bytes 1769476
  192.1 16.3 %copy-start.9 = (bf16[512,1024]{1,0:T(8,128)(2,1)S(1)}, bf16[512,1024]{1,0:T(8,128)(2,1)}, u32[]{:S(2)}) copy-start(bf16[512,1024]{1,0:T(8,128)(2,1)} %param.31) | copy-start | bytes 3145732
  218.2 17.5 %copy-start.8 = (bf16[1024,2048]{1,0:T(8,128)(2,1)S(1)}, bf16[1024,2048]{1,0:T(8,128)(2,1)}, u32[]{:S(2)}) copy-start(bf16[1024,2048]{1,0:T(8,128)(2,1)} %param.33) | copy-start | bytes 12582916
  218.2 26.6 %copy-start.2 = (bf16[128,2048]{1,0:T(8,128)(2,1)S(1)}, bf16[128,2048]{1,0:T(8,128)(2,1)}, u32[]{:S(2)}) copy-start(bf16[128,2048]{1,0:T(8,128)(2,1)} %param.17) | copy-start | bytes 1572868
  218.3 28.6 %copy-start.1 = (bf16[2048,512]{1,0:T(8,128)(2,1)S(1)}, bf16[2048,512]{1,0:T(8,128)(2,1)}, u32[]{:S(2)}) copy-start(bf16[2048,512]{1,0:T(8,128)(2,1)} %param.26) | copy-start | bytes 6291460
Sparse Core Ops, SparseCore 0:
  58.5 8.8 all-gather.3
  70.3 66.0 all-gather.5
  238.1 6.6 reduce-scatter.1
where the time goes:
time: 254 us; the launch traced here: 253 us
  matrix products  102 us (40%)
  blocking collectives  86.6 us (34%)
  other arithmetic  28.2 us (11%)
  waiting for transfers between devices  19.5 us (8%)
  between operations  13.4 us (5%)
  local copies, waits for them, and re-layouts  3.69 us (1%)
    all_gather x1, blocking collectives, body(): lax.all_gather(own_rope, ('sp', 'tp'), axis=0, tiled=True)  44.1 us
    psum x1, blocking collectives, body(): lax.psum((placed[0], placed[1], placed[2]), ('sp', 'tp'))  42.5 us
    dot_general x1, matrix products, fold_keys(): jnp.einsum('qhr,kr->hqk', query_rope, rope_keys, preferred_element_type=j...  27.8 us
    dot_general x1, matrix products, fold_keys(): jnp.einsum('qhd,khd->hqk', query_nope, keys, preferred_element_type=jnp.f...  18.4 us
    dot_general x1, matrix products, fold_keys(): jnp.einsum('hqk,khd->hqd', weights.astype(jnp.bfloat16), values, preferre...  17.5 us
    reduce_sum x1, other arithmetic, fold_keys(): total = jnp.sum(weights, axis=-1)  16.3 us
    all_gather x1, waiting for transfers between devices, body(): lax.all_gather(own_latents, ('sp', 'tp'), axis=0, tiled=True)  12.6 us
    dot_general x1, matrix products, body(): jnp.dot(pieces[0], w_value_up, preferred_element_type=jnp.float32)  9.87 us
  transfers between devices with their start and end apart: 3, of which 2 were waited for; matrix products, arithmetic and copies ran while one was open for 8% of the time, Pallas kernels for 0%

commit v1 on v0

--- a/solution.py
+++ b/solution.py
@@ -6,6 +6,11 @@
 GRID_W = 128
 EPS = 1e-06
 ROPE_BASE = 10000.0
+
+
+def axis_by_axis(x, one, other):
+    half = lax.psum(x, one)
+    return lax.psum(half, other)
 
 
 def modulate(rows_in, gain, shift, scale):
@@ -90,7 +95,7 @@
             for part in partials
         )
     )
-    shift, scale, gate = lax.psum((placed[0], placed[1], placed[2]), ("sp", "tp"))
+    shift, scale, gate = axis_by_axis((placed[0], placed[1], placed[2]), "tp", "sp")
     h_rows = modulate(latent, norm_gain, shift[0], scale[0])
     h_ctx = modulate(context, norm_gain, shift[1], scale[1])
     own_positions = sp_index * tok_dev + tp_index * rows + jnp.arange(rows, dtype=jnp.int32)

time: 254 us -> 291 us (1.15)
  blocking collectives: 86.6 us -> 123 us
    psum x1 -> x2, blocking collectives: 42.5 us -> 82.2 us  [the longest x1 78.4 us: axis_by_axis(): return lax.psum(half, other)]
    all_gather x1, blocking collectives: 44.1 us -> 40.7 us  [body(): lax.all_gather(own_rope, ('sp', 'tp'), axis=0, tiled=True)]
  transfers between devices with their start and end apart: 3 -> 3, of which waited for: 2 -> 2; matrix products, arithmetic and copies ran while one was open for 8% -> 7% of each run, Pallas kernels for 0% -> 0%
where the time goes in v1:
time: 291 us; the launch traced here: 290 us
  blocking collectives  123 us (42%)
  matrix products  102 us (35%)
  other arithmetic  28.2 us (10%)
  waiting for transfers between devices  20.5 us (7%)
  between operations  13.4 us (5%)
  local copies, waits for them, and re-layouts  3.7 us (1%)
    psum x1, blocking collectives, axis_by_axis(): return lax.psum(half, other)  78.4 us
    all_gather x1, blocking collectives, body(): lax.all_gather(own_rope, ('sp', 'tp'), axis=0, tiled=True)  40.7 us
    dot_general x1, matrix products, fold_keys(): jnp.einsum('qhr,kr->hqk', query_rope, rope_keys, preferred_element_type=j...  27.7 us
    dot_general x1, matrix products, fold_keys(): jnp.einsum('qhd,khd->hqk', query_nope, keys, preferred_element_type=jnp.f...  18.4 us
    dot_general x1, matrix products, fold_keys(): jnp.einsum('hqk,khd->hqd', weights.astype(jnp.bfloat16), values, preferre...  17.5 us
    reduce_sum x1, other arithmetic, fold_keys(): total = jnp.sum(weights, axis=-1)  16.3 us
    all_gather x1, waiting for transfers between devices, body(): lax.all_gather(own_latents, ('sp', 'tp'), axis=0, tiled=True)  13.6 us
    dot_general x1, matrix products, body(): jnp.dot(pieces[0], w_value_up, preferred_element_type=jnp.float32)  9.85 us
  transfers between devices with their start and end apart: 3, of which 2 were waited for; matrix products, arithmetic and copies ran while one was open for 7% of the time, Pallas kernels for 0%

profile of v1, /device:TPU:0, one launch (start us, length us, event | category | flops | bytes accessed | tf_op | source)
XLA Modules:
  0.0 290.4 jit_solution(8415639273513257800)
XLA Ops:
  6.5 0.0 copy-start
  6.5 0.0 copy-start.6
  6.5 0.0 copy-start.5
  6.5 0.0 copy-start.4
  6.5 0.0 copy-start.7
  6.5 0.0 all-gather.4.cloned.1.call-start
  6.6 0.9 divide_multiply_fusion.1
  7.5 0.7 divide_multiply_fusion
  8.2 1.2 fusion.17
  9.4 1.4 convolution_dynamic-update-slice_fusion.1
  10.9 1.4 convolution_dynamic-update-slice_fusion.2
  12.3 1.4 convolution_dynamic-update-slice_fusion
  13.8 3.9 %all-reduce.1 = (f32[2,2048]{1,0:T(2,128)S(1)}, f32[2,2048]{1,0:T(2,128)S(1)}, f32[2,2048]{1,0:T(2,128)S(1)}) all-reduce(f32[2,2048]{1,0:T(2,128)S(1)} %convolution_dynamic-update-slice_fusion, f32[2,2048]{1,0:T(2,128)S(1)} %convolution_dynamic-update-slice_fusion.1, ...), channel_id=1, replica_groups=mesh['sp'=16,'tp'=2] {'tp'}, use_global_device_ids=true, to_apply=%region_5.6 | all-reduce | flops 12288 | bytes 98304 | tf_op jit(solution)/shard_map/psum | solution.py:12
  17.6 78.4 %all-reduce = (f32[2,2048]{1,0:T(2,128)S(1)}, f32[2,2048]{1,0:T(2,128)S(1)}, f32[2,2048]{1,0:T(2,128)S(1)}) all-reduce(f32[2,2048]{1,0:T(2,128)S(1)} %get-tuple-element.8, f32[2,2048]{1,0:T(2,128)S(1)} %get-tuple-element.9, f32[2,2048]{1,0:T(2,128)S(1)} %get-tuple-element.10), channel_id=1, replica_groups=mesh['sp'=16,'tp'=2] {'sp'}, use_global_device_ids=true, to_apply=%region_6.7 | all-reduce | flops 12288 | bytes 98304 | tf_op jit(solution)/shard_map/psum | solution.py:13
  96.0 2.1 fusion.21
  98.1 0.0 all-gather.4.cloned.1.call-update
  98.2 0.0 all-gather.6.cloned.1.call-start
  98.2 2.3 multiply_reduce_fusion
  100.5 1.0 fusion.26
  101.5 2.3 multiply_reduce_fusion.1
  103.8 0.8 multiply_convert_fusion.1
  104.6 0.8 multiply_convert_fusion
  105.3 0.7 pad_maximum_fusion.1
  106.0 0.0 all-gather.6.cloned.1.call-update
  106.0 0.0 reduce-scatter.2.cloned.1.call-start
  106.1 0.1 multiply_bitcast_fusion.1
  106.2 0.0 copy-done.4
  106.2 1.3 fusion.55
  107.6 0.1 subtract_convert_fusion.1
  107.7 0.0 copy-done.6
  107.7 0.0 copy-done.5
  107.7 0.2 convolution_convert_fusion.4
  108.0 0.1 copy.49
  108.1 40.7 %all-gather = bf16[32,144,64]{1,2,0:T(8,128)(2,1)S(1)} all-gather(bf16[1,144,64]{1,2,0:T(8,128)(2,1)S(1)} %maximum_bitcast_fusion), channel_id=1, replica_groups=mesh['sp'=16,'tp'=2] {'sp','tp'}, dimensions={0}, use_global_device_ids=true | all-gather | bytes 608256 | tf_op jit(solution)/shard_map/all_gather | solution.py:149
  148.8 0.6 copy.50
  149.4 2.5 reshape.383
  151.9 0.1 broadcast_multiply_fusion.2
  152.0 0.1 fusion.32
  152.1 0.0 copy-done.7
  152.2 0.1 broadcast_multiply_fusion
  152.2 0.0 all-gather.4.cloned.1.call-done
  152.3 0.0 copy-done
  152.3 2.2 fusion.56
  154.4 0.3 reshape_reshape.4
  154.7 0.7 subtract_convert_fusion
  155.4 0.6 pad_maximum_fusion
  156.0 0.1 convert_element_type.105
  156.2 3.8 %fusion.10 = bf16[32,8,8,128]{3,2,1,0:T(8,128)(2,1)S(1)} fusion(bf16[256,2048]{1,0:T(8,128)(2,1)} %all-gather.4.cloned.1.call-done, bf16[2048,1024]{1,0:T(8,128)(2,1)} %param.25), kind=kOutput, calls=%fused_computation.16 | convolution fusion | flops 1074003968 | bytes 5767168 | tf_op jit(solution)/shard_map/dot_general | solution.py:112
  159.9 13.6 %all-gather.6.cloned.1.call-done = bf16[4608,512]{1,0:T(8,128)(2,1)} async-done(((bf16[144,512]{1,0:T(8,128)(2,1)}), bf16[4608,512]{1,0:T(8,128)(2,1)}) %all-gather.6.cloned.1.call-update) | async-done | bytes 4718608 | tf_op jit(solution)/shard_map/all_gather | solution.py:148
  173.5 9.4 %convolution_convert_fusion.1 = bf16[4608,1024]{0,1:T(8,128)(2,1)} fusion(bf16[4608,512]{1,0:T(8,128)(2,1)} %all-gather.6.cloned.1.call-done, bf16[512,1024]{1,0:T(8,128)(2,1)} %param.30), kind=kOutput, calls=%fused_computation.9 | convolution fusion | flops 4836556800 | bytes 15204352 | tf_op jit(solution)/shard_map/dot_general | solution.py:151
  183.0 18.4 %fusion.23 = f32[8,256,4608]{2,1,0:T(8,128)} fusion(bf16[4608,8,128]{0,2,1:T(8,128)(2,1)} %bitcast.68, bf16[32,8,8,128]{3,2,1,0:T(8,128)(2,1)S(1)} %fusion.10), kind=kOutput, calls=%fused_computation.29 | convolution fusion | flops 2415919104 | bytes 47710208 | tf_op jit(solution)/shard_map/qhd,khd->hqk/dot_general | solution.py:127
  201.4 0.0 copy-done.3
  201.4 27.7 %fusion.54 = (f32[8,256]{1,0:T(8,128)S(1)}, f32[8,256,4608]{2,1,0:T(8,128)}) fusion(f32[8,4608]{1,0:T(8,128)S(1)} %broadcast_multiply_fusion, f32[8,256,4608]{2,1,0:T(8,128)} %fusion.23, bf16[4608,64,1]{0,1,2:T(8,128)(2,1)S(1)} %copy-done.3, bf16[256,8,64]{0,2,1:T(8,128)(2,1)S(1)} %convert_element_type.105), kind=kOutput, calls=%fused_computation.103 | convolution fusion | flops 1245706240 | bytes 76505088 | tf_op jit(solution)/shard_map/qhr,kr->hqk/dot_general | solution.py:128
  229.1 16.3 %fusion.2 = f32[8,256]{1,0:T(8,128)S(1)} fusion(f32[8,256,4608]{2,1,0:T(8,128)} %get-tuple-element.32, f32[8,256]{1,0:T(8,128)S(1)} %broadcast_maximum_fusion), kind=kLoop, calls=%fused_computation.4 | loop fusion | flops 18872320 | bytes 37765120 | tf_op jit(solution)/shard_map/reduce_sum | solution.py:136
  245.4 0.0 copy-done.9
  245.4 9.9 %convolution_convert_fusion = bf16[4608,1024]{0,1:T(8,128)(2,1)} fusion(bf16[4608,512]{1,0:T(8,128)(2,1)} %all-gather.6.cloned.1.call-done, bf16[512,1024]{1,0:T(8,128)(2,1)S(1)} %copy-done.9), kind=kOutput, calls=%fused_computation.8 | convolution fusion | flops 4836556800 | bytes 15204352 | tf_op jit(solution)/shard_map/dot_general | solution.py:152
  255.3 17.5 %fusion.14 = bf16[256,8,128]{0,2,1:T(8,128)(2,1)S(1)} fusion(bf16[4608,8,128]{0,2,1:T(8,128)(2,1)} %bitcast.67, f32[8,256,4608]{2,1,0:T(8,128)} %get-tuple-element.32, f32[8,256]{1,0:T(8,128)S(1)} %broadcast_maximum_fusion, f32[256,8]{0,1:T(8,128)S(1)} %bitcast.70), kind=kOutput, calls=%fused_computation.18 | convolution fusion | flops 2435317760 | bytes 47726592 | tf_op jit(solution)/shard_map/hqk,khd->hqd/dot_general | solution.py:137
  272.8 0.0 copy-done.8
  272.8 2.2 convolution_convert_fusion.2
  275.0 0.0 reduce-scatter.2.cloned.1.call-update
  275.1 6.8 %reduce-scatter.2.cloned.1.call-done = bf16[128,2048]{1,0:T(8,128)(2,1)} async-done(((bf16[256,2048]{1,0:T(8,128)(2,1)}), bf16[128,2048]{1,0:T(8,128)(2,1)}) %reduce-scatter.2.cloned.1.call-update) | async-done | bytes 524304 | tf_op jit(solution)/shard_map/reduce_scatter | solution.py:157
  281.9 0.0 copy-done.2
  281.9 2.0 fusion.22
  283.9 0.0 copy-done.1
  (23 shorter events, 0.2 us)
Async XLA Ops:
  6.5 145.7 %copy-start = (bf16[2048,512]{1,0:T(8,128)(2,1)S(1)}, bf16[2048,512]{1,0:T(8,128)(2,1)}, u32[]{:S(2)}) copy-start(bf16[2048,512]{1,0:T(8,128)(2,1)} %param.26) | copy-start | bytes 6291460
  6.5 101.2 %copy-start.6 = (f32[2048]{0:T(1024)S(1)}, f32[2048]{0:T(1024)}, u32[]{:S(2)}) copy-start(f32[2048]{0:T(1024)} %param.24) | copy-start | bytes 24580
  6.5 101.2 %copy-start.5 = (bf16[16,2048]{1,0:T(8,128)(2,1)S(1)}, bf16[16,2048]{1,0:T(8,128)(2,1)}, u32[]{:S(2)}) copy-start(bf16[16,2048]{1,0:T(8,128)(2,1)} %param.20) | copy-start | bytes 196612
  6.5 99.7 %copy-start.4 = (bf16[2048,64]{0,1:T(8,128)(2,1)S(1)}, bf16[2048,64]{0,1:T(8,128)(2,1)}, u32[]{:S(2)}) copy-start(bf16[2048,64]{0,1:T(8,128)(2,1)} %param.28) | copy-start | bytes 786436
  6.5 145.6 %copy-start.7 = (f32[8]{0:T(128)S(1)}, f32[8]{0:T(128)}, u32[]{:S(2)}) copy-start(f32[8]{0:T(128)} %param.32) | copy-start | bytes 100
  6.5 145.7 %all-gather.4.cloned.1.call-start = ((), (), s32[]{:S(2)}) async-start(), calls=%async_computation.1 | async-start | bytes 1572864 | tf_op jit(solution)/shard_map/all_gather | solution.py:110
  98.2 75.4 %all-gather.6.cloned.1.call-start = ((), (), s32[]{:S(2)}) async-start(), calls=%async_computation.2 | async-start | bytes 4866048 | tf_op jit(solution)/shard_map/all_gather | solution.py:148
  106.0 175.9 %reduce-scatter.2.cloned.1.call-start = ((), (), s32[]{:S(2)}) async-start(), calls=%async_computation.3 | async-start | bytes 1572864 | tf_op jit(solution)/shard_map/reduce_scatter | solution.py:157
  183.0 18.4 %copy-start.3 = (bf16[4608,64,1]{0,1,2:T(8,128)(2,1)S(1)}, bf16[4608,64,1]{0,1,2:T(8,128)(2,1)}, u32[]{:S(2)}) copy-start(bf16[4608,64,1]{0,1,2:T(8,128)(2,1)} %reshape.383) | copy-start | bytes 1769476
  229.1 16.3 %copy-start.9 = (bf16[512,1024]{1,0:T(8,128)(2,1)S(1)}, bf16[512,1024]{1,0:T(8,128)(2,1)}, u32[]{:S(2)}) copy-start(bf16[512,1024]{1,0:T(8,128)(2,1)} %param.31) | copy-start | bytes 3145732
  255.3 17.5 %copy-start.8 = (bf16[1024,2048]{1,0:T(8,128)(2,1)S(1)}, bf16[1024,2048]{1,0:T(8,128)(2,1)}, u32[]{:S(2)}) copy-start(bf16[1024,2048]{1,0:T(8,128)(2,1)} %param.33) | copy-start | bytes 12582916
  255.3 26.6 %copy-start.2 = (bf16[128,2048]{1,0:T(8,128)(2,1)S(1)}, bf16[128,2048]{1,0:T(8,128)(2,1)}, u32[]{:S(2)}) copy-start(bf16[128,2048]{1,0:T(8,128)(2,1)} %param.17) | copy-start | bytes 1572868
  255.3 28.6 %copy-start.1 = (bf16[2048,512]{1,0:T(8,128)(2,1)S(1)}, bf16[2048,512]{1,0:T(8,128)(2,1)}, u32[]{:S(2)}) copy-start(bf16[2048,512]{1,0:T(8,128)(2,1)} %param.26) | copy-start | bytes 6291460
Sparse Core Ops, SparseCore 0:
  98.3 4.8 all-gather.3
  106.2 67.3 all-gather.5
  275.2 6.6 reduce-scatter.1
